TPU v7x, 32 devices: a whole 2x2x4 slice. The times are simulated.
32 devices in a mesh: rep: 2 (over x), fs: 8 (over z, y), tp: 2 (over core).
Axes of the slice: x: 2, y: 2, z: 4, core: 2. Of those that a mesh axis runs over, the one named last changes fastest.
Arguments:
- tokens: bfloat16 [10240, 2048], P(('rep', 'fs', 'tp')), may hold values from -6 to 6
- mix_gain: float32 [2048], replicated, may hold values from 0.1 to 1.9
- w_bgate: bfloat16 [2048, 2048], P('fs', 'tp'), may hold values from -0.125 to 0.125
- w_cgate: bfloat16 [2048, 2048], P('fs', 'tp'), may hold values from -0.125 to 0.125
- w_value: bfloat16 [2048, 2048], P('fs', 'tp'), may hold values from -0.125 to 0.125
- conv_taps: float32 [3, 2048], replicated, may hold values from -3 to 3
- w_mixout: bfloat16 [2048, 2048], P('tp', 'fs'), may hold values from -0.125 to 0.125
- mlp_gain: float32 [2048], replicated, may hold values from 0.1 to 1.9
- w_gate: bfloat16 [2048, 2816], P('fs', 'tp'), may hold values from -0.125 to 0.125
- w_up: bfloat16 [2048, 2816], P('fs', 'tp'), may hold values from -0.125 to 0.125
- w_down: bfloat16 [2816, 2048], P('tp', 'fs'), may hold values from -0.109375 to 0.109375
Outputs:
- block_out: bfloat16 [10240, 2048], P(('rep', 'fs', 'tp'))
All inputs are finite; a program needn't handle non-finite values.
Results may differ from a plain program's by a relative error of at most 0.0085.
Values may be sent and summed in bfloat16 or wider, within the bound.
A program may use at most 128 MiB of HBM per device.

v0:
```python
import jax
import jax.numpy as jnp
from jax import lax
from jax.sharding import PartitionSpec as P


def rms_scale(matrix, gain):
    values = matrix.astype(jnp.float32)
    factor = lax.rsqrt(jnp.mean(values * values, axis=-1, keepdims=True) + 1e-06)
    return values * factor * gain


def causal_taps(mixed, filters):
    length = mixed.shape[-2]
    widths = [(0, 0)] * (mixed.ndim - 2) + [(2, 0), (0, 0)]
    padded = jnp.pad(mixed, widths)
    return (
        filters[0] * padded[..., 0:length, :]
        + filters[1] * padded[..., 1 : length + 1, :]
        + filters[2] * padded[..., 2 : length + 2, :]
    )


def gather_rows(normed):
    return lax.all_gather(normed, "tp", axis=0, tiled=True)


def project_in(gathered, stacked):
    return jnp.einsum(
        "td,kdc->ktc",
        gathered,
        lax.all_gather(stacked, "fs", axis=1, tiled=True),
        preferred_element_type=jnp.float32,
    )


def collect_out(weight):
    return lax.all_gather(weight, "fs", axis=1, tiled=True)


def sum_parts(local_cols, weight):
    return lax.psum_scatter(
        jnp.dot(local_cols, weight, preferred_element_type=jnp.float32).astype(jnp.bfloat16),
        "tp",
        scatter_dimension=0,
        tiled=True,
    ).astype(jnp.float32)


def on_device(
    tokens, mix_gain, w_bgate, w_cgate, w_value, conv_taps, w_mixout, mlp_gain, w_gate, w_up, w_down
):
    normed = rms_scale(tokens, mix_gain).astype(jnp.bfloat16)
    gathered = gather_rows(normed)
    projected = project_in(gathered, jnp.stack([w_bgate, w_cgate, w_value])).astype(jnp.bfloat16)
    channels = projected.shape[2]
    channel_taps = lax.dynamic_slice_in_dim(conv_taps, lax.axis_index("tp") * channels, channels, 1)
    mixed_in = projected[1].astype(jnp.float32) * projected[2].astype(jnp.float32)
    gated = (projected[0].astype(jnp.float32) * causal_taps(mixed_in, channel_taps)).astype(
        jnp.bfloat16
    )
    residual = tokens.astype(jnp.float32) + sum_parts(gated, collect_out(w_mixout))
    normed_two = rms_scale(residual, mlp_gain).astype(jnp.bfloat16)
    gathered_two = gather_rows(normed_two)
    gate_up = project_in(gathered_two, jnp.stack([w_gate, w_up]))
    hidden = (jax.nn.silu(gate_up[0]) * gate_up[1]).astype(jnp.bfloat16)
    result = residual + 0.5 * sum_parts(hidden, collect_out(w_down))
    return result.astype(jnp.bfloat16)


def solution(mesh):
    return jax.shard_map(
        on_device,
        mesh=mesh,
        in_specs=(
            P(("rep", "fs", "tp"), None),
            P(),
            P("fs", "tp"),
            P("fs", "tp"),
            P("fs", "tp"),
            P(),
            P("tp", "fs"),
            P(),
            P("fs", "tp"),
            P("fs", "tp"),
            P("tp", "fs"),
        ),
        out_specs=P(("rep", "fs", "tp"), None),
        check_vma=False,
    )
```

profile of v0, /device:TPU:0, one launch (start us, length us, event | category | flops | bytes accessed | tf_op | source)
XLA Modules:
  0.0 599.1 jit_solution(9736600943579483417)
XLA Ops:
  6.5 0.0 all-gather.9.cloned.1.call-start
  6.5 0.0 copy-start.5
  6.5 0.0 copy-start.6
  6.5 0.0 copy-start.7
  6.5 1.8 fusion.2
  8.3 2.7 fusion.4
  11.1 0.0 all-gather.9.cloned.1.call-update
  11.1 0.0 all-gather.7.cloned.1.call-start
  11.2 0.0 copy-done.5
  11.2 0.0 copy-done.6
  11.2 0.0 copy-done.7
  11.2 1.3 pad_maximum_fusion
  12.5 0.0 all-gather.7.cloned.1.call-update
  12.5 0.0 all-gather.11.cloned.1.call-start
  12.6 0.7 all-gather.11.cloned.1.call-update
  13.3 0.0 reduce-scatter.3.cloned.1.call-start
  13.3 0.9 constant_dynamic-slice_fusion
  14.2 11.1 %all-gather.9.cloned.1.call-done = bf16[640,2048]{1,0:T(8,128)(2,1)} async-done(((bf16[320,2048]{1,0:T(8,128)(2,1)}), bf16[640,2048]{1,0:T(8,128)(2,1)}) %all-gather.9.cloned.1.call-update) | async-done | bytes 2621456 | tf_op jit(solution)/shard_map/all_gather | solution.py:25
  25.3 179.5 %all-gather.7.cloned.1.call-done = bf16[3,2048,1024]{2,1,0:T(8,128)(2,1)} async-done(((bf16[3,256,1024]{2,1,0:T(8,128)(2,1)}), bf16[3,2048,1024]{2,1,0:T(8,128)(2,1)}) %all-gather.7.cloned.1.call-update) | async-done | bytes 12582928 | tf_op jit(solution)/shard_map/all_gather | solution.py:32
  204.8 12.0 %convert_bitcast_fusion = bf16[3,640,1024]{2,1,0:T(8,128)(2,1)S(1)} fusion(bf16[3,2048,1024]{2,1,0:T(8,128)(2,1)} %all-gather.7.cloned.1.call-done, bf16[640,2048]{1,0:T(8,128)(2,1)} %all-gather.9.cloned.1.call-done), kind=kOutput, calls=%fused_computation.1 | convolution fusion | flops 8055029760 | bytes 19136512 | tf_op jit(solution)/shard_map/td,kdc->ktc/dot_general | solution.py:29
  216.9 0.0 copy-start.2
  216.9 1.9 copy-done.2
  218.7 0.5 multiply_bitcast_fusion
  219.2 60.5 %all-gather.11.cloned.1.call-done = bf16[1024,2048]{1,0:T(8,128)(2,1)} async-done(((bf16[1024,256]{1,0:T(8,128)(2,1)}), bf16[1024,2048]{1,0:T(8,128)(2,1)}) %all-gather.11.cloned.1.call-update) | async-done | bytes 4194320 | tf_op jit(solution)/shard_map/all_gather | solution.py:38
  279.7 7.4 %convolution_convert_fusion.1 = bf16[640,2048]{1,0:T(8,128)(2,1)} fusion(bf16[1024,2048]{1,0:T(8,128)(2,1)} %all-gather.11.cloned.1.call-done, f32[640,1024]{1,0:T(8,128)S(1)} %multiply_bitcast_fusion, bf16[3,640,1024]{2,1,0:T(8,128)(2,1)} %copy-done.2, f32[1024]{0:T(1024)S(1)} %bitcast.51, f32[1024]{0:T(1024)S(1)} %bitcast.50, f32[1024]{0:T(1024)S(1)} %bitcast.49), kind=kOutput, calls=%fused_computation.10 | convolution fusion | flops 2690908160 | bytes 10760192 | tf_op jit(solution)/shard_map/dot_general | solution.py:43
  287.1 0.0 copy-start.3
  287.1 0.0 copy-start.4
  287.1 0.0 reduce-scatter.3.cloned.1.call-update
  287.1 0.0 all-gather.13.cloned.1.call-start
  287.2 1.0 copy-done.3
  288.2 0.3 copy.12
  288.5 0.0 copy-done.4
  288.5 0.0 copy-start
  288.5 0.3 copy.13
  288.8 1.3 pad_maximum_fusion.1
  290.1 0.0 copy-start.8
  290.1 0.0 all-gather.13.cloned.1.call-update
  290.1 0.0 all-gather.15.cloned.1.call-start
  290.2 5.7 reduce-scatter.3.cloned.1.call-done
  295.9 0.0 copy-done
  295.9 0.0 copy-start.1
  295.9 1.9 multiply_reduce_fusion
  297.9 0.0 copy-done.8
  297.9 0.0 copy-done.1
  297.9 1.6 multiply_convert_fusion
  299.5 0.0 all-gather.15.cloned.1.call-update
  299.5 0.0 all-gather.17.cloned.1.call-start
  299.6 0.7 all-gather.17.cloned.1.call-update
  300.3 0.2 reduce-scatter.5.cloned.1.call-start
  300.5 161.9 %all-gather.13.cloned.1.call-done = bf16[2,2048,1408]{1,2,0:T(8,128)(2,1)} async-done(((bf16[2,256,1408]{1,2,0:T(8,128)(2,1)}), bf16[2,2048,1408]{1,2,0:T(8,128)(2,1)}) %all-gather.13.cloned.1.call-update) | async-done | bytes 11534352 | tf_op jit(solution)/shard_map/all_gather | solution.py:32
  462.4 11.0 %all-gather.15.cloned.1.call-done = bf16[640,2048]{1,0:T(8,128)(2,1)} async-done(((bf16[320,2048]{1,0:T(8,128)(2,1)}), bf16[640,2048]{1,0:T(8,128)(2,1)}) %all-gather.15.cloned.1.call-update) | async-done | bytes 2621456 | tf_op jit(solution)/shard_map/all_gather | solution.py:25
  473.4 14.6 %convolution_bitcast_fusion = f32[2,640,1408]{1,2,0:T(8,128)} fusion(bf16[2,2048,1408]{1,2,0:T(8,128)(2,1)} %all-gather.13.cloned.1.call-done, bf16[640,2048]{1,0:T(8,128)(2,1)} %all-gather.15.cloned.1.call-done), kind=kOutput, calls=%fused_computation | convolution fusion | flops 7381975040 | bytes 21364736 | tf_op jit(solution)/shard_map/td,kdc->ktc/dot_general | solution.py:29
  488.0 81.8 %all-gather.17.cloned.1.call-done = bf16[1408,2048]{1,0:T(8,128)(2,1)} async-done(((bf16[1408,256]{1,0:T(8,128)(2,1)}), bf16[1408,2048]{1,0:T(8,128)(2,1)}) %all-gather.17.cloned.1.call-update) | async-done | bytes 5767184 | tf_op jit(solution)/shard_map/all_gather | solution.py:38
  569.8 10.7 %convolution_convert_fusion = bf16[640,2048]{1,0:T(8,128)(2,1)} fusion(bf16[1408,2048]{1,0:T(8,128)(2,1)} %all-gather.17.cloned.1.call-done, f32[2,640,1408]{1,2,0:T(8,128)} %convolution_bitcast_fusion), kind=kOutput, calls=%fused_computation.9 | convolution fusion | flops 3697704960 | bytes 15597568 | tf_op jit(solution)/shard_map/dot_general | solution.py:43
  580.4 0.0 reduce-scatter.5.cloned.1.call-update
  580.5 8.8 %reduce-scatter.5.cloned.1.call-done = bf16[320,2048]{1,0:T(8,128)(2,1)} async-done(((bf16[640,2048]{1,0:T(8,128)(2,1)}), bf16[320,2048]{1,0:T(8,128)(2,1)}) %reduce-scatter.5.cloned.1.call-update) | async-done | bytes 1310736 | tf_op jit(solution)/shard_map/reduce_scatter | solution.py:42
  589.3 3.1 add_convert_fusion
  (2 shorter events, 0.0 us)
Async XLA Ops:
  6.5 18.8 %all-gather.9.cloned.1.call-start = ((), (), s32[]{:S(2)}) async-start(), calls=%async_computation.3 | async-start | bytes 3932160 | tf_op jit(solution)/shard_map/all_gather | solution.py:25
  6.5 4.6 copy-start.5
  6.5 4.6 copy-start.6
  6.5 4.6 copy-start.7
  11.1 193.7 %all-gather.7.cloned.1.call-start = ((), (), s32[]{:S(2)}) async-start(), calls=%async_computation.2 | async-start | bytes 14155776 | tf_op jit(solution)/shard_map/all_gather | solution.py:32
  12.5 267.2 %all-gather.11.cloned.1.call-start = ((), (), s32[]{:S(2)}) async-start(), calls=%async_computation.4 | async-start | bytes 4718592 | tf_op jit(solution)/shard_map/all_gather | solution.py:38
  13.3 282.6 %reduce-scatter.3.cloned.1.call-start = ((), (), s32[]{:S(2)}) async-start(), calls=%async_computation.5 | async-start | bytes 3932160 | tf_op jit(solution)/shard_map/reduce_scatter | solution.py:42
  216.9 1.9 copy-start.2
  287.1 1.1 copy-start.3
  287.1 1.4 copy-start.4
  287.1 175.3 %all-gather.13.cloned.1.call-start = ((), (), s32[]{:S(2)}) async-start(), calls=%async_computation.6 | async-start | bytes 12976128 | tf_op jit(solution)/shard_map/all_gather | solution.py:32
  288.5 7.4 %copy-start = (bf16[320,2048]{1,0:T(8,128)(2,1)S(1)}, bf16[320,2048]{1,0:T(8,128)(2,1)}, u32[]{:S(2)}) copy-start(bf16[320,2048]{1,0:T(8,128)(2,1)} %param.11) | copy-start | bytes 3932164
  290.1 7.8 %copy-start.8 = (f32[2048]{0:T(1024)S(1)}, f32[2048]{0:T(1024)}, u32[]{:S(2)}) copy-start(f32[2048]{0:T(1024)} %param.18) | copy-start | bytes 24580
  290.1 183.3 %all-gather.15.cloned.1.call-start = ((), (), s32[]{:S(2)}) async-start(), calls=%async_computation.7 | async-start | bytes 3932160 | tf_op jit(solution)/shard_map/all_gather | solution.py:25
  295.9 2.0 copy-start.1
  299.5 270.3 %all-gather.17.cloned.1.call-start = ((), (), s32[]{:S(2)}) async-start(), calls=%async_computation.8 | async-start | bytes 6488064 | tf_op jit(solution)/shard_map/all_gather | solution.py:38
  300.3 289.0 %reduce-scatter.5.cloned.1.call-start = ((), (), s32[]{:S(2)}) async-start(), calls=%async_computation.9 | async-start | bytes 3932160 | tf_op jit(solution)/shard_map/reduce_scatter | solution.py:42
Sparse Core Ops, SparseCore 0:
  11.2 14.0 all-gather.8
  27.5 177.2 all-gather.6
  206.9 72.7 all-gather.10
  287.2 8.6 reduce-scatter.2
  297.8 164.5 all-gather.12
  463.8 9.5 all-gather.14
  475.4 94.3 all-gather.16
  580.6 8.6 reduce-scatter.4
where the time goes:
time: 599 us
  waiting for transfers between devices  522 us (87%)
  matrix products  44.7 us (7%)
  other arithmetic  14.3 us (2%)
  between operations  13.6 us (2%)
    all_gather x2, waiting for transfers between devices, project_in(): lax.all_gather(stacked, 'fs', axis=1, tiled=True)  341 us
    all_gather x2, waiting for transfers between devices, collect_out(): return lax.all_gather(weight, 'fs', axis=1, tiled=True)  142 us
    dot_general x2, matrix products, project_in(): jnp.einsum('td,kdc->ktc', gathered, lax.all_gather(stacked, 'fs', axis=1,...  26.7 us
    all_gather x2, waiting for transfers between devices, gather_rows(): return lax.all_gather(normed, 'tp', axis=0, tiled=True)  22 us
    dot_general x2, matrix products, sum_parts(): jnp.dot(local_cols, weight, preferred_element_type=jnp.float32)  18 us
    reduce_scatter x2, waiting for transfers between devices, sum_parts(): lax.psum_scatter(jnp.dot(local_cols, weight, preferred_element_type=jnp.f...  14.5 us
  transfers between devices with their start and end apart: 8, of which 8 were waited for; matrix products, arithmetic and copies ran while one was open for 6% of the time, Pallas kernels for 0%

commit v1 on v0

--- a/solution.py
+++ b/solution.py
@@ -26,11 +26,37 @@
 
 
 def project_in(gathered, stacked):
-    return jnp.einsum(
-        "td,kdc->ktc",
-        gathered,
-        lax.all_gather(stacked, "fs", axis=1, tiled=True),
-        preferred_element_type=jnp.float32,
+
+    def obtain_the_teams(tile_in, ndim_at, local):
+        along_axis = "fs"
+        near = jax.lax.axis_size(along_axis)
+        current_value, p_next, row_out = (
+            near,
+            jax.lax.axis_index(along_axis),
+            tile_in.shape[ndim_at],
+        )
+        xs_all = tuple(((h, (h + 1) % current_value) for h in range(current_value)))
+        inbox = tuple(((h, (h - 1) % current_value) for h in range(current_value)))
+        w2 = current_value // 2
+        all_rows = base_arr = tile_in
+        y1 = local(tile_in, p_next * row_out)
+        for i in [*range(1, w2 + 1)]:
+            all_rows = jax.lax.ppermute(all_rows, along_axis, xs_all)
+            if i < current_value - w2:
+                base_arr = jax.lax.ppermute(base_arr, along_axis, inbox)
+                y1 = y1 + local(base_arr, (p_next + i) % current_value * row_out)
+            y1 = y1 + local(all_rows, (p_next - i) % current_value * row_out)
+        return y1
+
+    return obtain_the_teams(
+        stacked,
+        1,
+        lambda part, offset: jnp.einsum(
+            "td,kdc->ktc",
+            lax.dynamic_slice_in_dim(gathered, offset, part.shape[1], axis=1),
+            part,
+            preferred_element_type=jnp.float32,
+        ),
     )
 
 

time: 599 us -> 656 us (1.095)
  matrix products: 44.7 us -> 127 us
  waiting for transfers between devices: 522 us -> 456 us
  starting transfers between devices: 0.47 us -> 35 us
    ppermute x0 -> x14, waiting for transfers between devices: none -> 437 us  [the longest x8 423 us: obtain_the_teams(): all_rows = jax.lax.ppermute(all_rows, along_axis, xs_all)]
    all_gather x2 -> x0, waiting for transfers between devices: 341 us -> none  [project_in(): lax.all_gather(stacked, 'fs', axis=1, tiled=True)]
    all_gather x2, waiting for transfers between devices: 142 us -> 0.01 us  [collect_out(): return lax.all_gather(weight, 'fs', axis=1, tiled=True)]
    dot_general x2 -> x16, matrix products: 26.7 us -> 106 us  [project_in(): jnp.einsum('td,kdc->ktc', lax.dynamic_slice_in_dim(gathered, offset, part...]
    ppermute x0 -> x14, starting transfers between devices: none -> 34.8 us  [the longest x8 19.9 us: obtain_the_teams(): all_rows = jax.lax.ppermute(all_rows, along_axis, xs_all)]
    all_gather x2, waiting for transfers between devices: 22 us -> 0.02 us  [gather_rows(): return lax.all_gather(normed, 'tp', axis=0, tiled=True)]
  transfers between devices with their start and end apart: 8 -> 20, of which waited for: 8 -> 11; matrix products, arithmetic and copies ran while one was open for 6% -> 18% of each run, Pallas kernels for 0% -> 0%
where the time goes in v1:
time: 656 us; the launch traced here: 655 us
  waiting for transfers between devices  456 us (70%)
  matrix products  127 us (19%)
  starting transfers between devices  35 us (5%)
  other arithmetic  15.8 us (2%)
  between operations  13.6 us (2%)
  local copies, waits for them, and re-layouts  7.58 us (1%)
    ppermute x8, waiting for transfers between devices, obtain_the_teams(): all_rows = jax.lax.ppermute(all_rows, along_axis, xs_all)  423 us
    dot_general x16, matrix products, project_in(): jnp.einsum('td,kdc->ktc', lax.dynamic_slice_in_dim(gathered, offset, part...  106 us
    dot_general x2, matrix products, sum_parts(): jnp.dot(local_cols, weight, preferred_element_type=jnp.float32)  20.6 us
    ppermute x8, starting transfers between devices, obtain_the_teams(): all_rows = jax.lax.ppermute(all_rows, along_axis, xs_all)  19.9 us
    reduce_scatter x2, waiting for transfers between devices, sum_parts(): lax.psum_scatter(jnp.dot(local_cols, weight, preferred_element_type=jnp.f...  18.2 us
    ppermute x6, starting transfers between devices, obtain_the_teams(): base_arr = jax.lax.ppermute(base_arr, along_axis, inbox)  14.9 us
    ppermute x6, waiting for transfers between devices, obtain_the_teams(): base_arr = jax.lax.ppermute(base_arr, along_axis, inbox)  14.6 us
  transfers between devices with their start and end apart: 20, of which 11 were waited for; matrix products, arithmetic and copies ran while one was open for 18% of the time, Pallas kernels for 0%

profile of v1, /device:TPU:0, one launch (start us, length us, event | category | flops | bytes accessed | tf_op | source)
XLA Modules:
  0.0 655.1 jit_solution(10982762843762781919)
XLA Ops:
  6.5 1.8 fusion.3
  8.3 2.7 fusion.5
  11.1 0.0 all-gather.5.cloned.1.call-update
  11.1 0.0 all-gather.7.cloned.1.call-start
  11.2 1.4 pad_maximum_fusion
  12.6 3.0 collective-permute-start.1
  15.6 3.0 collective-permute-start
  18.6 64.6 %collective-permute-done.1 = bf16[3,256,1024]{2,1,0:T(8,128)(2,1)S(1)} collective-permute-done((bf16[3,256,1024]{2,1,0:T(8,128)(2,1)}, bf16[3,256,1024]{2,1,0:T(8,128)(2,1)S(1)}, u32[]{:S(2)}, u32[]{:S(2)}) %collective-permute-start.1) | collective-permute-done | bytes 1572896 | tf_op jit(solution)/shard_map/ppermute | solution.py:44
  83.2 2.4 collective-permute-start.3
  85.6 0.0 all-gather.7.cloned.1.call-update
  85.6 0.0 reduce-scatter.3.cloned.1.call-start
  85.7 3.1 collective-permute-start.2
  88.8 76.0 %collective-permute-done.3 = bf16[3,256,1024]{2,1,0:T(8,128)(2,1)S(1)} collective-permute-done((bf16[3,256,1024]{2,1,0:T(8,128)(2,1)S(1)}, bf16[3,256,1024]{2,1,0:T(8,128)(2,1)S(1)}, u32[]{:S(2)}, u32[]{:S(2)}) %collective-permute-start.3) | collective-permute-done | bytes 1572896 | tf_op jit(solution)/shard_map/ppermute | solution.py:44
  164.8 2.5 collective-permute-start.5
  167.3 0.9 constant_dynamic-slice_fusion
  168.2 0.0 all-gather.5.cloned.1.call-done
  168.2 2.3 fusion.37
  170.6 5.8 fusion.39
  176.4 3.1 collective-permute-start.4
  179.5 4.3 fusion.41
  183.8 63.8 %collective-permute-done.5 = bf16[3,256,1024]{2,1,0:T(8,128)(2,1)} collective-permute-done((bf16[3,256,1024]{2,1,0:T(8,128)(2,1)S(1)}, bf16[3,256,1024]{2,1,0:T(8,128)(2,1)}, u32[]{:S(2)}, u32[]{:S(2)}) %collective-permute-start.5) | collective-permute-done | bytes 1572896 | tf_op jit(solution)/shard_map/ppermute | solution.py:44
  247.6 2.6 collective-permute-start.6
  250.2 4.3 fusion.33
  254.5 5.8 fusion.35
  260.3 5.7 fusion.29
  266.0 4.4 fusion.31
  270.3 15.7 %collective-permute-done.6 = bf16[3,256,1024]{2,1,0:T(8,128)(2,1)} collective-permute-done((bf16[3,256,1024]{2,1,0:T(8,128)(2,1)}, bf16[3,256,1024]{2,1,0:T(8,128)(2,1)}, u32[]{:S(2)}, u32[]{:S(2)}) %collective-permute-start.6) | collective-permute-done | bytes 1572896 | tf_op jit(solution)/shard_map/ppermute | solution.py:44
  286.0 16.3 %fusion = bf16[3,640,1024]{2,1,0:T(8,128)(2,1)S(1)} fusion(f32[3,1024,640]{1,2,0:T(8,128)} %fusion.29, f32[3,1024,640]{1,2,0:T(8,128)} %fusion.31, f32[3,1024,640]{1,2,0:T(8,128)} %fusion.33, f32[3,1024,640]{1,2,0:T(8,128)} %fusion.35, f32[3,1024,640]{1,2,0:T(8,128)S(1)} %fusion.37, f32[3,1024,640]{1,2,0:T(8,128)} %fusion.41, f32[3,1024,640]{1,2,0:T(8,128)} %fusion.39, ...), kind=kOutput, calls=%fused_computation.2 | convolution fusion | flops 1022361600 | bytes 60882948 | tf_op jit(solution)/shard_map/td,kdc->ktc/dot_general | solution.py:54
  302.3 1.8 copy-done.2
  304.2 2.1 multiply_bitcast_fusion
  306.2 9.7 %convolution_convert_fusion.1 = bf16[640,2048]{1,0:T(8,128)(2,1)} fusion(bf16[1024,2048]{1,0:T(8,128)(2,1)} %all-gather.7.cloned.1.call-done, f32[640,1024]{1,0:T(8,128)} %multiply_bitcast_fusion, bf16[3,640,1024]{2,1,0:T(8,128)(2,1)} %copy-done.2, f32[1024]{0:T(1024)S(1)} %bitcast.108, f32[1024]{0:T(1024)S(1)} %bitcast.107, f32[1024]{0:T(1024)S(1)} %bitcast.106), kind=kOutput, calls=%fused_computation.11 | convolution fusion | flops 2690908160 | bytes 10760192 | tf_op jit(solution)/shard_map/dot_general | solution.py:69
  315.9 0.0 all-gather.9.cloned.1.call-start
  316.0 9.0 %reduce-scatter.3.cloned.1.call-done = bf16[320,2048]{1,0:T(8,128)(2,1)} async-done(((bf16[640,2048]{1,0:T(8,128)(2,1)}), bf16[320,2048]{1,0:T(8,128)(2,1)}) %reduce-scatter.3.cloned.1.call-update) | async-done | bytes 1310736 | tf_op jit(solution)/shard_map/reduce_scatter | solution.py:68
  325.0 1.9 multiply_reduce_fusion
  326.9 1.6 multiply_convert_fusion
  328.6 0.0 all-gather.11.cloned.1.call-start
  328.6 0.5 all-gather.11.cloned.1.call-update
  329.2 0.0 reduce-scatter.5.cloned.1.call-start
  329.2 1.4 copy.12
  330.6 2.2 copy.13
  332.8 1.2 pad_maximum_fusion.1
  334.1 1.9 collective-permute-start.8
  336.0 2.9 collective-permute-start.7
  338.9 66.9 %collective-permute-done.8 = bf16[2,256,1408]{1,2,0:T(8,128)(2,1)S(1)} collective-permute-done((bf16[2,256,1408]{1,2,0:T(8,128)(2,1)S(1)}, bf16[2,256,1408]{1,2,0:T(8,128)(2,1)S(1)}, u32[]{:S(2)}, u32[]{:S(2)}) %collective-permute-start.8) | collective-permute-done | bytes 1441824 | tf_op jit(solution)/shard_map/ppermute | solution.py:44
  405.8 2.5 collective-permute-start.10
  408.3 1.1 copy-done.12
  409.4 2.8 collective-permute-start.9
  412.2 88.0 %collective-permute-done.10 = bf16[2,256,1408]{1,2,0:T(8,128)(2,1)S(1)} collective-permute-done((bf16[2,256,1408]{1,2,0:T(8,128)(2,1)S(1)}, bf16[2,256,1408]{1,2,0:T(8,128)(2,1)S(1)}, u32[]{:S(2)}, u32[]{:S(2)}) %collective-permute-start.10) | collective-permute-done | bytes 1441824 | tf_op jit(solution)/shard_map/ppermute | solution.py:44
  500.2 2.5 collective-permute-start.12
  502.7 12.1 %collective-permute-done.9 = bf16[2,256,1408]{1,2,0:T(8,128)(2,1)} collective-permute-done((bf16[2,256,1408]{1,2,0:T(8,128)(2,1)S(1)}, bf16[2,256,1408]{1,2,0:T(8,128)(2,1)}, u32[]{:S(2)}, u32[]{:S(2)}) %collective-permute-start.9) | collective-permute-done | bytes 1441824 | tf_op jit(solution)/shard_map/ppermute | solution.py:46
  514.7 47.8 %collective-permute-done.12 = bf16[2,256,1408]{1,2,0:T(8,128)(2,1)} collective-permute-done((bf16[2,256,1408]{1,2,0:T(8,128)(2,1)S(1)}, bf16[2,256,1408]{1,2,0:T(8,128)(2,1)}, u32[]{:S(2)}, u32[]{:S(2)}) %collective-permute-start.12) | collective-permute-done | bytes 1441824 | tf_op jit(solution)/shard_map/ppermute | solution.py:44
  562.5 2.6 collective-permute-start.13
  565.1 5.8 fusion.18
  570.9 5.8 fusion.20
  576.7 4.2 fusion.22
  580.9 4.2 fusion.26
  585.2 4.3 fusion.24
  589.4 5.6 fusion.14
  595.0 2.6 collective-permute-done.11
  597.6 5.6 fusion.16
  603.2 21.8 %add_bitcast_fusion = f32[2,640,1408]{1,2,0:T(8,128)} fusion(f32[2,1408,640]{2,1,0:T(8,128)} %fusion.14, f32[2,1408,640]{2,1,0:T(8,128)} %fusion.16, f32[2,1408,640]{2,1,0:T(8,128)} %fusion.18, f32[2,1408,640]{2,1,0:T(8,128)} %fusion.20, f32[2,1408,640]{2,1,0:T(8,128)} %fusion.22, f32[2,1408,640]{2,1,0:T(8,128)} %fusion.26, f32[2,1408,640]{2,1,0:T(8,128)} %fusion.24, ...), kind=kOutput, calls=%fused_computation.1 | convolution fusion | flops 935362560 | bytes 59441156 | tf_op jit(solution)/shard_map/td,kdc->ktc/dot_general | solution.py:54
  625.0 10.9 %convolution_convert_fusion = bf16[640,2048]{1,0:T(8,128)(2,1)} fusion(bf16[1408,2048]{1,0:T(8,128)(2,1)} %all-gather.11.cloned.1.call-done, f32[2,640,1408]{1,2,0:T(8,128)} %add_bitcast_fusion), kind=kOutput, calls=%fused_computation.10 | convolution fusion | flops 3697704960 | bytes 15597568 | tf_op jit(solution)/shard_map/dot_general | solution.py:69
  636.0 9.2 %reduce-scatter.5.cloned.1.call-done = bf16[320,2048]{1,0:T(8,128)(2,1)} async-done(((bf16[640,2048]{1,0:T(8,128)(2,1)}), bf16[320,2048]{1,0:T(8,128)(2,1)}) %reduce-scatter.5.cloned.1.call-update) | async-done | bytes 1310736 | tf_op jit(solution)/shard_map/reduce_scatter | solution.py:68
  645.2 3.1 add_convert_fusion.1
  (49 shorter events, 0.2 us)
Async XLA Ops:
  6.5 4.6 copy-start.6
  6.5 4.6 copy-start.8
  6.5 4.6 copy-start.10
  6.5 161.7 %all-gather.5.cloned.1.call-start = ((), (), s32[]{:S(2)}) async-start(), calls=%async_computation.2 | async-start | bytes 3932160 | tf_op jit(solution)/shard_map/all_gather | solution.py:25
  11.1 295.1 %all-gather.7.cloned.1.call-start = ((), (), s32[]{:S(2)}) async-start(), calls=%async_computation.3 | async-start | bytes 4718592 | tf_op jit(solution)/shard_map/all_gather | solution.py:64
  12.6 70.7 %collective-permute-start.1 = (bf16[3,256,1024]{2,1,0:T(8,128)(2,1)}, bf16[3,256,1024]{2,1,0:T(8,128)(2,1)S(1)}, u32[]{:S(2)}, u32[]{:S(2)}) collective-permute-start(bf16[3,256,1024]{2,1,0:T(8,128)(2,1)} %pad_maximum_fusion), channel_id=1, source_target_pairs={{0,2},{2,4},{4,6},{6,8},{8,10},{10,12},{12,14},{14,0},{1,3},{3,5},... | collective-permute-start | bytes 4718600 | tf_op jit(solution)/shard_map/ppermute | solution.py:44
  15.6 70.1 %collective-permute-start = (bf16[3,256,1024]{2,1,0:T(8,128)(2,1)}, bf16[3,256,1024]{2,1,0:T(8,128)(2,1)}, u32[]{:S(2)}, u32[]{:S(2)}) collective-permute-start(bf16[3,256,1024]{2,1,0:T(8,128)(2,1)} %pad_maximum_fusion), channel_id=1, source_target_pairs={{0,14},{2,0},{4,2},{6,4},{8,6},{10,8},{12,10},{14,12},{1,15},{3,1}... | collective-permute-start | bytes 4718600 | tf_op jit(solution)/shard_map/ppermute | solution.py:46
  83.2 81.6 %collective-permute-start.3 = (bf16[3,256,1024]{2,1,0:T(8,128)(2,1)S(1)}, bf16[3,256,1024]{2,1,0:T(8,128)(2,1)S(1)}, u32[]{:S(2)}, u32[]{:S(2)}) collective-permute-start(bf16[3,256,1024]{2,1,0:T(8,128)(2,1)S(1)} %collective-permute-done.1), channel_id=1, source_target_pairs={{0,2},{2,4},{4,6},{6,8},{8,10},{10,12},{12,14},{14,0},{1,3},{3,5},... | collective-permute-start | bytes 4718600 | tf_op jit(solution)/shard_map/ppermute | solution.py:44
  85.6 239.3 %reduce-scatter.3.cloned.1.call-start = ((), (), s32[]{:S(2)}) async-start(), calls=%async_computation.4 | async-start | bytes 3932160 | tf_op jit(solution)/shard_map/reduce_scatter | solution.py:68
  85.7 90.7 %collective-permute-start.2 = (bf16[3,256,1024]{2,1,0:T(8,128)(2,1)}, bf16[3,256,1024]{2,1,0:T(8,128)(2,1)}, u32[]{:S(2)}, u32[]{:S(2)}) collective-permute-start(bf16[3,256,1024]{2,1,0:T(8,128)(2,1)} %collective-permute-done), channel_id=1, source_target_pairs={{0,14},{2,0},{4,2},{6,4},{8,6},{10,8},{12,10},{14,12},{1,15},{3,1}... | collective-permute-start | bytes 4718600 | tf_op jit(solution)/shard_map/ppermute | solution.py:46
  164.8 82.8 %collective-permute-start.5 = (bf16[3,256,1024]{2,1,0:T(8,128)(2,1)S(1)}, bf16[3,256,1024]{2,1,0:T(8,128)(2,1)}, u32[]{:S(2)}, u32[]{:S(2)}) collective-permute-start(bf16[3,256,1024]{2,1,0:T(8,128)(2,1)S(1)} %collective-permute-done.3), channel_id=1, source_target_pairs={{0,2},{2,4},{4,6},{6,8},{8,10},{10,12},{12,14},{14,0},{1,3},{3,5},... | collective-permute-start | bytes 4718600 | tf_op jit(solution)/shard_map/ppermute | solution.py:44
  168.2 2.3 copy-start.4
  170.5 8.9 %copy-start.7 = (bf16[256,1024]{1,0:T(8,128)(2,1)S(1)}, bf16[256,1024]{1,0:T(8,128)(2,1)}, u32[]{:S(2)}) copy-start(bf16[256,1024]{1,0:T(8,128)(2,1)} %param.15) | copy-start | bytes 1572868
  170.6 8.9 %copy-start.9 = (bf16[256,1024]{1,0:T(8,128)(2,1)S(1)}, bf16[256,1024]{1,0:T(8,128)(2,1)}, u32[]{:S(2)}) copy-start(bf16[256,1024]{1,0:T(8,128)(2,1)} %param.14) | copy-start | bytes 1572868
  170.6 8.9 %copy-start.11 = (bf16[256,1024]{1,0:T(8,128)(2,1)S(1)}, bf16[256,1024]{1,0:T(8,128)(2,1)}, u32[]{:S(2)}) copy-start(bf16[256,1024]{1,0:T(8,128)(2,1)} %param.13) | copy-start | bytes 1572868
  176.4 89.6 %collective-permute-start.4 = (bf16[3,256,1024]{2,1,0:T(8,128)(2,1)}, bf16[3,256,1024]{2,1,0:T(8,128)(2,1)S(1)}, u32[]{:S(2)}, u32[]{:S(2)}) collective-permute-start(bf16[3,256,1024]{2,1,0:T(8,128)(2,1)} %collective-permute-done.2), channel_id=1, source_target_pairs={{0,14},{2,0},{4,2},{6,4},{8,6},{10,8},{12,10},{14,12},{1,15},{3,1}... | collective-permute-start | bytes 4718600 | tf_op jit(solution)/shard_map/ppermute | solution.py:46
  247.6 38.4 %collective-permute-start.6 = (bf16[3,256,1024]{2,1,0:T(8,128)(2,1)}, bf16[3,256,1024]{2,1,0:T(8,128)(2,1)}, u32[]{:S(2)}, u32[]{:S(2)}) collective-permute-start(bf16[3,256,1024]{2,1,0:T(8,128)(2,1)} %collective-permute-done.5), channel_id=1, source_target_pairs={{0,2},{2,4},{4,6},{6,8},{8,10},{10,12},{12,14},{14,0},{1,3},{3,5},... | collective-permute-start | bytes 4718600 | tf_op jit(solution)/shard_map/ppermute | solution.py:44
  302.3 1.9 copy-start.2
  315.9 9.1 %copy-start = (bf16[320,2048]{1,0:T(8,128)(2,1)S(1)}, bf16[320,2048]{1,0:T(8,128)(2,1)}, u32[]{:S(2)}) copy-start(bf16[320,2048]{1,0:T(8,128)(2,1)} %param.11) | copy-start | bytes 3932164
  315.9 11.0 %copy-start.17 = (f32[2048]{0:T(1024)S(1)}, f32[2048]{0:T(1024)}, u32[]{:S(2)}) copy-start(f32[2048]{0:T(1024)} %param.18) | copy-start | bytes 24580
  315.9 249.2 %all-gather.9.cloned.1.call-start = ((), (), s32[]{:S(2)}) async-start(), calls=%async_computation.5 | async-start | bytes 3932160 | tf_op jit(solution)/shard_map/all_gather | solution.py:25
  325.0 2.0 copy-start.1
  328.6 296.4 %all-gather.11.cloned.1.call-start = ((), (), s32[]{:S(2)}) async-start(), calls=%async_computation.6 | async-start | bytes 6488064 | tf_op jit(solution)/shard_map/all_gather | solution.py:64
  329.2 316.0 %reduce-scatter.5.cloned.1.call-start = ((), (), s32[]{:S(2)}) async-start(), calls=%async_computation.7 | async-start | bytes 3932160 | tf_op jit(solution)/shard_map/reduce_scatter | solution.py:68
  334.1 71.7 %collective-permute-start.8 = (bf16[2,256,1408]{1,2,0:T(8,128)(2,1)S(1)}, bf16[2,256,1408]{1,2,0:T(8,128)(2,1)S(1)}, u32[]{:S(2)}, u32[]{:S(2)}) collective-permute-start(bf16[2,256,1408]{1,2,0:T(8,128)(2,1)S(1)} %pad_maximum_fusion.1), channel_id=1, source_target_pairs={{0,2},{2,4},{4,6},{6,8},{8,10},{10,12},{12,14},{14,0},{1,3},{3,5},... | collective-permute-start | bytes 4325384 | tf_op jit(solution)/shard_map/ppermute | solution.py:44
  336.0 72.3 %collective-permute-start.7 = (bf16[2,256,1408]{1,2,0:T(8,128)(2,1)S(1)}, bf16[2,256,1408]{1,2,0:T(8,128)(2,1)S(1)}, u32[]{:S(2)}, u32[]{:S(2)}) collective-permute-start(bf16[2,256,1408]{1,2,0:T(8,128)(2,1)S(1)} %pad_maximum_fusion.1), channel_id=1, source_target_pairs={{0,14},{2,0},{4,2},{6,4},{8,6},{10,8},{12,10},{14,12},{1,15},{3,1}... | collective-permute-start | bytes 4325384 | tf_op jit(solution)/shard_map/ppermute | solution.py:46
  405.8 108.9 %copy-start.14 = (bf16[2,256,1408]{1,2,0:T(8,128)(2,1)}, bf16[2,256,1408]{1,2,0:T(8,128)(2,1)S(1)}, u32[]{:S(2)}) copy-start(bf16[2,256,1408]{1,2,0:T(8,128)(2,1)S(1)} %collective-permute-done.8) | copy-start | bytes 4325380
  405.8 94.4 %collective-permute-start.10 = (bf16[2,256,1408]{1,2,0:T(8,128)(2,1)S(1)}, bf16[2,256,1408]{1,2,0:T(8,128)(2,1)S(1)}, u32[]{:S(2)}, u32[]{:S(2)}) collective-permute-start(bf16[2,256,1408]{1,2,0:T(8,128)(2,1)S(1)} %collective-permute-done.8), channel_id=1, source_target_pairs={{0,2},{2,4},{4,6},{6,8},{8,10},{10,12},{12,14},{14,0},{1,3},{3,5},... | collective-permute-start | bytes 4325384 | tf_op jit(solution)/shard_map/ppermute | solution.py:44
  408.3 1.1 copy-start.12
  409.4 105.3 %collective-permute-start.9 = (bf16[2,256,1408]{1,2,0:T(8,128)(2,1)S(1)}, bf16[2,256,1408]{1,2,0:T(8,128)(2,1)}, u32[]{:S(2)}, u32[]{:S(2)}) collective-permute-start(bf16[2,256,1408]{1,2,0:T(8,128)(2,1)S(1)} %collective-permute-done.7), channel_id=1, source_target_pairs={{0,14},{2,0},{4,2},{6,4},{8,6},{10,8},{12,10},{14,12},{1,15},{3,1}... | collective-permute-start | bytes 4325384 | tf_op jit(solution)/shard_map/ppermute | solution.py:46
  500.2 14.5 %copy-start.16 = (bf16[2,256,1408]{1,2,0:T(8,128)(2,1)}, bf16[2,256,1408]{1,2,0:T(8,128)(2,1)S(1)}, u32[]{:S(2)}) copy-start(bf16[2,256,1408]{1,2,0:T(8,128)(2,1)S(1)} %collective-permute-done.10) | copy-start | bytes 4325380
  500.2 62.3 %collective-permute-start.12 = (bf16[2,256,1408]{1,2,0:T(8,128)(2,1)S(1)}, bf16[2,256,1408]{1,2,0:T(8,128)(2,1)}, u32[]{:S(2)}, u32[]{:S(2)}) collective-permute-start(bf16[2,256,1408]{1,2,0:T(8,128)(2,1)S(1)} %collective-permute-done.10), channel_id=1, source_target_pairs={{0,2},{2,4},{4,6},{6,8},{8,10},{10,12},{12,14},{14,0},{1,3},{3,5},... | collective-permute-start | bytes 4325384 | tf_op jit(solution)/shard_map/ppermute | solution.py:44
  514.7 82.8 %collective-permute-start.11 = (bf16[2,256,1408]{1,2,0:T(8,128)(2,1)}, bf16[2,256,1408]{1,2,0:T(8,128)(2,1)}, u32[]{:S(2)}, u32[]{:S(2)}) collective-permute-start(bf16[2,256,1408]{1,2,0:T(8,128)(2,1)} %collective-permute-done.9), channel_id=1, source_target_pairs={{0,14},{2,0},{4,2},{6,4},{8,6},{10,8},{12,10},{14,12},{1,15},{3,1}... | collective-permute-start | bytes 4325384 | tf_op jit(solution)/shard_map/ppermute | solution.py:46
  562.5 40.7 %collective-permute-start.13 = (bf16[2,256,1408]{1,2,0:T(8,128)(2,1)}, bf16[2,256,1408]{1,2,0:T(8,128)(2,1)}, u32[]{:S(2)}, u32[]{:S(2)}) collective-permute-start(bf16[2,256,1408]{1,2,0:T(8,128)(2,1)} %collective-permute-done.12), channel_id=1, source_target_pairs={{0,2},{2,4},{4,6},{6,8},{8,10},{10,12},{12,14},{14,0},{1,3},{3,5},... | collective-permute-start | bytes 4325384 | tf_op jit(solution)/shard_map/ppermute | solution.py:44
  565.1 5.8 copy-start.5
  570.9 5.8 copy-start.15
  576.7 4.2 copy-start.3
  580.9 4.3 copy-start.13
Sparse Core Ops, SparseCore 0:
  11.2 14.0 all-gather.4
  85.8 155.2 all-gather.6
  316.0 8.8 reduce-scatter.2
  328.7 12.6 all-gather.8
  343.3 203.4 all-gather.10
  636.1 9.0 reduce-scatter.4
